TPU v7x, 32 devices: a whole 2x2x4 slice. The times are simulated.
32 devices in a mesh: sp: 8 (over z, x), tp: 4 (over y, core).
Axes of the slice: x: 2, y: 2, z: 4, core: 2. Of those that a mesh axis runs over, the one named last changes fastest.
Arguments:
- inputs: bfloat16 [3072, 4096], P('sp', 'tp'), may hold values from -40 to 40, as said below
- query_weight: bfloat16 [2, 4096, 1024], P(None, None, 'tp'), may hold values from -0.2 to 0.2
- key_weight: bfloat16 [2, 4096, 1024], P(None, None, 'tp'), may hold values from -0.2 to 0.2
- value_weight: bfloat16 [4096, 2048], P(None, 'tp'), may hold values from -0.09375 to 0.09375
- pool_weight: bfloat16 [4096, 2048], P(None, 'tp'), may hold values from -0.09375 to 0.09375
- mix_lambda: float32 [16], P('tp'), may hold values from 0.3 to 0.8
- head_gain: float32 [128], replicated, may hold values from 0.1 to 1.9
- attn_out_weight: bfloat16 [2048, 4096], P('tp'), may hold values from -0.125 to 0.125
- pool_out_weight: bfloat16 [2048, 4096], P('tp'), may hold values from -0.125 to 0.125
Outputs:
- mixed: bfloat16 [3072, 4096], P(('sp', 'tp'))
- log_totals: float32 [2, 16, 3072], P(None, 'tp', 'sp')
Inputs may be any that keep to these rules, and one draw needn't show every extreme that they name: inputs of order one, in some draws a few rows larger.
All inputs are finite; a program needn't handle non-finite values.
Results may differ from a plain program's by a relative error of at most 0.015.
Values may be sent and summed in bfloat16 or wider, within the bound.
A program may use at most 192 MiB of HBM per device.

v0:
```python
import jax
import jax.numpy as jnp
from jax import lax
from jax.sharding import PartitionSpec as P

HEAD_DIM = 64
POOL_WIDTH = 2048


def extended(value, sides, width):
    for axis, dim in sides:
        count, length = (lax.axis_size(axis), value.shape[dim])
        up = [(i, (i + 1) % count) for i in range(count - 1)]
        down = [(j, i) for i, j in up]
        last = lax.slice_in_dim(value, length - width, length, axis=dim)
        first = lax.slice_in_dim(value, 0, width, axis=dim)
        before = lax.ppermute(last, axis, up)
        after = lax.ppermute(first, axis, down)
        value = jnp.concatenate([before, value, after], axis=dim)
    return value


def on_device(
    inputs,
    query_weight,
    key_weight,
    value_weight,
    pool_weight,
    mix_lambda,
    head_gain,
    attn_out_weight,
    pool_out_weight,
):
    tok_rows = inputs.shape[0]
    width = query_weight.shape[2]
    heads_here = width // HEAD_DIM
    piece = lax.all_gather(inputs, "tp", axis=1, tiled=True)
    query_sum = jnp.einsum("td,mdc->tmc", piece, query_weight, preferred_element_type=jnp.float32)
    key_sum = jnp.einsum("td,mdc->tmc", piece, key_weight, preferred_element_type=jnp.float32)
    value_sum = jnp.dot(piece, value_weight, preferred_element_type=jnp.float32)
    pool_sum = jnp.dot(piece, pool_weight, preferred_element_type=jnp.float32)
    queries = query_sum.astype(jnp.bfloat16).reshape(tok_rows, 2, heads_here, HEAD_DIM)
    keys = key_sum.astype(jnp.bfloat16)
    values = value_sum.astype(jnp.bfloat16)
    pool_in = pool_sum.astype(jnp.bfloat16)
    key_piece = lax.all_gather(keys, "sp", axis=0, tiled=True)
    value_piece = lax.all_gather(values, "sp", axis=0, tiled=True)
    rows = key_piece.shape[0]
    key_heads = key_piece.reshape(rows, 2, heads_here, HEAD_DIM)
    value_heads = value_piece.reshape(rows, heads_here, 2 * HEAD_DIM)
    running_max = jnp.full((2, heads_here, tok_rows), -1e30, jnp.float32)
    scores = jnp.einsum(
        "qmhd,kmhd->mhqk", queries, key_heads, preferred_element_type=jnp.float32
    ) * HEAD_DIM ** (-0.5)
    new_max = jnp.maximum(running_max, jnp.max(scores, axis=-1))
    expo = jnp.exp(scores - new_max[..., None])
    totals = jnp.sum(expo, axis=-1)
    numer = jnp.einsum(
        "mhqk,khe->mhqe", expo.astype(jnp.bfloat16), value_heads, preferred_element_type=jnp.float32
    )
    running_max, totals, numer = (new_max, totals, numer)
    log_totals = running_max + jnp.log(totals)
    diff = (
        numer[0] / totals[0][..., None]
        - mix_lambda[:, None, None] * numer[1] / totals[1][..., None]
    )
    scaled = diff * lax.rsqrt(jnp.mean(diff * diff, axis=-1, keepdims=True) + 1e-05) * head_gain
    attention_attn = (
        jnp.transpose(scaled, (1, 0, 2))
        .reshape(tok_rows, heads_here * 2 * HEAD_DIM)
        .astype(jnp.bfloat16)
    )
    attn, log_totals = (attention_attn, log_totals)
    padded = extended(pool_in, (("sp", 0),), 8).astype(jnp.float32)
    channels = pool_in.shape[1]
    total_tok = tok_rows * lax.axis_size("sp")
    position = lax.axis_index("sp") * tok_rows + jnp.arange(tok_rows, dtype=jnp.int32)
    group = (lax.axis_index("tp") * channels + jnp.arange(channels, dtype=jnp.int32)) // (
        POOL_WIDTH // 4
    )
    result = jnp.zeros((tok_rows, channels), jnp.float32)
    for group_index, reach in enumerate((2, 4, 8, 16)):
        radius = reach // 2
        window_sum = padded[8 - radius : 8 - radius + tok_rows]
        for shift_by in range(-radius + 1, radius):
            window_sum = window_sum + padded[8 + shift_by : 8 + shift_by + tok_rows]
        low = jnp.clip(position - radius, 0, total_tok)
        high = jnp.clip(position + radius, 0, total_tok)
        window_mean = window_sum / (high - low).astype(jnp.float32)[:, None]
        result = jnp.where((group == group_index)[None, :], window_mean, result)
    pooled = (result - pool_in.astype(jnp.float32)).astype(jnp.bfloat16)
    mixed = lax.psum_scatter(
        (
            jnp.dot(attn, attn_out_weight, preferred_element_type=jnp.float32)
            + jnp.dot(pooled, pool_out_weight, preferred_element_type=jnp.float32)
        ).astype(jnp.bfloat16),
        "tp",
        scatter_dimension=0,
        tiled=True,
    )
    return (mixed, log_totals)


def solution(mesh):
    in_specs = (
        P("sp", "tp"),
        P(None, None, "tp"),
        P(None, None, "tp"),
        P(None, "tp"),
        P(None, "tp"),
        P("tp"),
        P(),
        P("tp", None),
        P("tp", None),
    )
    out_specs = (P(("sp", "tp"), None), P(None, "tp", "sp"))
    return jax.shard_map(
        on_device, mesh=mesh, in_specs=in_specs, out_specs=out_specs, check_vma=False
    )
```

profile of v0, /device:TPU:0, one launch (start us, length us, event | category | flops | bytes accessed | tf_op | source)
XLA Modules:
  0.0 232.9 jit_solution(1138345739911840571)
XLA Ops:
  7.2 0.0 all-gather.4.cloned.1.call-start
  7.2 0.7 all-gather.4.cloned.1.call-update
  7.9 0.0 all-gather.8.cloned.1.call-start
  7.9 32.9 %all-gather.4.cloned.1.call-done = bf16[384,4096]{1,0:T(8,128)(2,1)} async-done(((bf16[384,1024]{1,0:T(8,128)(2,1)}), bf16[384,4096]{1,0:T(8,128)(2,1)}) %all-gather.4.cloned.1.call-update) | async-done | bytes 3145744 | tf_op jit(solution)/shard_map/all_gather | solution.py:37
  40.8 5.8 %fusion.14 = bf16[384,2,256]{2,0,1:T(8,128)(2,1)} fusion(bf16[2,4096,256]{2,1,0:T(8,128)(2,1)} %param.11, bf16[384,4096]{1,0:T(8,128)(2,1)} %all-gather.4.cloned.1.call-done), kind=kOutput, calls=%fused_computation.13 | convolution fusion | flops 1610809344 | bytes 7733248 | tf_op jit(solution)/shard_map/td,mdc->tmc/dot_general | solution.py:39
  46.6 0.0 all-gather.8.cloned.1.call-update
  46.6 0.0 all-gather.6.cloned.1.call-start
  46.7 0.6 broadcast_compare_fusion
  47.3 0.6 broadcast_compare_fusion.2
  47.9 0.6 subtract_convert_fusion
  48.5 0.6 subtract_convert_fusion.2
  49.1 0.0 copy-done.11
  49.1 4.7 %convolution_convert_fusion.1 = bf16[384,512]{1,0:T(8,128)(2,1)} fusion(bf16[384,4096]{1,0:T(8,128)(2,1)S(1)} %copy-done.11, bf16[4096,512]{1,0:T(8,128)(2,1)} %param.12), kind=kOutput, calls=%fused_computation.15 | convolution fusion | flops 1610809344 | bytes 7733248 | tf_op jit(solution)/shard_map/dot_general | solution.py:40
  53.8 0.0 all-gather.6.cloned.1.call-update
  53.8 0.0 reduce-scatter.2.cloned.1.call-start
  53.9 0.0 copy-start.9
  53.9 4.3 %convolution_convert_fusion = bf16[384,512]{1,0:T(8,128)(2,1)S(1)} fusion(bf16[384,4096]{1,0:T(8,128)(2,1)S(1)} %copy-done.11, bf16[4096,512]{1,0:T(8,128)(2,1)} %param.13), kind=kOutput, calls=%fused_computation.14 | convolution fusion | flops 1610809344 | bytes 7733248 | tf_op jit(solution)/shard_map/dot_general | solution.py:41
  58.3 0.0 copy-start.2
  58.3 3.3 %collective-permute-start = (bf16[8,512]{1,0:T(8,128)(2,1)S(1)}, bf16[8,512]{1,0:T(8,128)(2,1)S(1)}, u32[]{:S(2)}, u32[]{:S(2)}) collective-permute-start(bf16[8,512]{1,0:T(8,128)(2,1)S(1)} %get-tuple-element.6), channel_id=1, source_target_pairs={{0,4},{4,8},{8,12},{12,16},{16,20},{20,24},{24,28},{1,5},{5,9},{9,... | collective-permute-start | bytes 24584 | tf_op jit(solution)/shard_map/ppermute | solution.py:17
  61.6 1.3 collective-permute-start.1
  62.9 0.0 copy-done.9
  62.9 2.4 %fusion.11 = bf16[384,2,256]{0,2,1:T(8,128)(2,1)S(1)} fusion(bf16[2,4096,256]{2,1,0:T(8,128)(2,1)S(1)} %copy-done.9, bf16[384,4096]{1,0:T(8,128)(2,1)S(1)} %copy-done.11), kind=kOutput, calls=%fused_computation.12 | convolution fusion | flops 1610809344 | bytes 7733248 | tf_op jit(solution)/shard_map/td,mdc->tmc/dot_general | solution.py:38
  65.3 0.0 collective-permute-done
  65.4 1.8 collective-permute-done.1
  67.2 0.0 copy-done.2
  67.2 1.0 maximum_convert_fusion
  68.2 38.6 %all-gather.8.cloned.1.call-done = bf16[3072,2,256]{2,0,1:T(8,128)(2,1)} async-done(((bf16[384,2,256]{2,0,1:T(8,128)(2,1)}), bf16[3072,2,256]{2,0,1:T(8,128)(2,1)}) %all-gather.8.cloned.1.call-update) | async-done | bytes 3145744 | tf_op jit(solution)/shard_map/all_gather | solution.py:46
  106.8 3.2 %copy.17 = bf16[3072,2,256]{0,2,1:T(8,128)(2,1)S(1)} copy(bf16[3072,2,256]{2,0,1:T(8,128)(2,1)} %all-gather.8.cloned.1.call-done) | data formatting | bytes 6291456 | tf_op jit(solution)/shard_map/all_gather | solution.py:46
  110.0 15.1 %multiply_reduce_fusion = (f32[2,4,384]{2,1,0:T(4,128)S(1)}, f32[2,4,384,3072]{3,2,1,0:T(8,128)}) fusion(bf16[384,2,4,64]{0,3,2,1:T(8,128)(2,1)S(1)} %bitcast.58, bf16[3072,2,4,64]{0,3,2,1:T(8,128)(2,1)S(1)} %bitcast.55), kind=kOutput, calls=%fused_computation.1 | convolution fusion | flops 1226830848 | bytes 41299968 | tf_op jit(solution)/shard_map/qmhd,kmhd->mhqk/dot_general | solution.py:52
  125.1 23.4 %fusion.1 = (bf16[2,4,384,3072]{3,2,1,0:T(8,128)(2,1)}, f32[2,4,384]{2,1,0:T(4,128)S(1)}) fusion(f32[2,4,384,3072]{3,2,1,0:T(8,128)} %get-tuple-element.11, f32[2,4,384]{2,1,0:T(4,128)S(1)} %broadcast_maximum_fusion), kind=kLoop, calls=%fused_computation.3 | loop fusion | flops 37745664 | bytes 56647680 | tf_op jit(solution)/shard_map/convert_element_type | solution.py:59
  148.6 19.2 %all-gather.6.cloned.1.call-done = bf16[3072,512]{1,0:T(8,128)(2,1)} async-done(((bf16[384,512]{1,0:T(8,128)(2,1)}), bf16[3072,512]{1,0:T(8,128)(2,1)}) %all-gather.6.cloned.1.call-update) | async-done | bytes 3145744 | tf_op jit(solution)/shard_map/all_gather | solution.py:47
  167.7 3.2 %copy.23 = bf16[3072,512]{0,1:T(8,128)(2,1)S(1)} copy(bf16[3072,512]{1,0:T(8,128)(2,1)} %all-gather.6.cloned.1.call-done) | data formatting | bytes 6291456 | tf_op jit(solution)/shard_map/reshape | solution.py:50
  170.9 0.0 copy-start.7
  170.9 0.0 copy-start.8
  171.0 0.0 copy-start
  171.0 10.3 %fusion.8 = f32[2,4,384,128]{2,3,0,1:T(8,128)S(1)} fusion(bf16[3072,4,128,1]{0,2,3,1:T(8,128)(2,1)S(1)} %bitcast.56, bf16[2,4,384,3072]{3,2,1,0:T(8,128)(2,1)} %get-tuple-element.4), kind=kOutput, calls=%fused_computation.11 | convolution fusion | flops 2415919104 | bytes 23592960 | tf_op jit(solution)/shard_map/mhqk,khe->mhqe/dot_general | solution.py:58
  181.3 0.0 copy-done.7
  181.3 0.2 multiply_reduce_fusion.1
  181.6 0.0 copy-done.8
  181.6 0.1 multiply_convert_fusion
  181.7 0.0 copy-done
  181.7 0.0 copy-start.1
  181.7 0.0 copy-start.3
  181.7 0.0 copy-start.4
  181.7 0.0 copy-start.5
  181.8 0.0 copy-start.6
  181.8 0.0 copy-start.10
  181.8 0.0 copy-start.12
  181.8 0.0 copy-start.13
  181.8 0.0 copy-start.14
  181.8 0.0 copy-start.15
  181.8 1.9 fusion.49
  183.7 0.0 copy-done.1
  183.7 0.0 copy-done.3
  183.7 0.0 copy-done.4
  183.8 0.0 copy-done.5
  183.8 0.0 copy-done.6
  183.8 0.5 copy-done.10
  184.3 0.0 copy-done.12
  184.3 0.0 copy-done.15
  184.3 5.3 %add_convert_fusion = bf16[384,4096]{1,0:T(8,128)(2,1)} fusion(f32[384,4096]{1,0:T(8,128)S(1)} %fusion.49, bf16[512,4096]{1,0:T(8,128)(2,1)S(1)} %copy-done.10, bf16[384,512]{1,0:T(8,128)(2,1)S(1)} %copy-done.3, f32[400,512]{1,0:T(8,128)S(1)} %copy-done.1, f32[384]{0:T(512)S(1)} %get-tuple-element.12, f32[384]{0:T(512)S(1)} %copy-done.4, ...), kind=kOutput, calls=%fused_computation.6 | convolution fusion | flops 1621032960 | bytes 26617856 | tf_op jit(solution)/shard_map/dot_general | solution.py:95
  189.6 0.0 reduce-scatter.2.cloned.1.call-update
  189.6 0.6 log_add_fusion
  190.3 36.1 %reduce-scatter.2.cloned.1.call-done = bf16[96,4096]{1,0:T(8,128)(2,1)} async-done(((bf16[384,4096]{1,0:T(8,128)(2,1)}), bf16[96,4096]{1,0:T(8,128)(2,1)}) %reduce-scatter.2.cloned.1.call-update) | async-done | bytes 786448 | tf_op jit(solution)/shard_map/reduce_scatter | solution.py:92
  (7 shorter events, 0.0 us)
Async XLA Ops:
  7.2 33.6 %all-gather.4.cloned.1.call-start = ((), (), s32[]{:S(2)}) async-start(), calls=%async_computation.1 | async-start | bytes 3932160 | tf_op jit(solution)/shard_map/all_gather | solution.py:37
  7.9 98.9 %all-gather.8.cloned.1.call-start = ((), (), s32[]{:S(2)}) async-start(), calls=%async_computation.3 | async-start | bytes 3538944 | tf_op jit(solution)/shard_map/all_gather | solution.py:46
  40.8 8.3 %copy-start.11 = (bf16[384,4096]{1,0:T(8,128)(2,1)S(1)}, bf16[384,4096]{1,0:T(8,128)(2,1)}, u32[]{:S(2)}) copy-start(bf16[384,4096]{1,0:T(8,128)(2,1)} %all-gather.4.cloned.1.call-done) | copy-start | bytes 9437188
  46.6 121.1 %all-gather.6.cloned.1.call-start = ((), (), s32[]{:S(2)}) async-start(), calls=%async_computation.2 | async-start | bytes 3538944 | tf_op jit(solution)/shard_map/all_gather | solution.py:47
  53.8 172.5 %reduce-scatter.2.cloned.1.call-start = ((), (), s32[]{:S(2)}) async-start(), calls=%async_computation.4 | async-start | bytes 3932160 | tf_op jit(solution)/shard_map/reduce_scatter | solution.py:92
  53.9 9.0 %copy-start.9 = (bf16[2,4096,256]{2,1,0:T(8,128)(2,1)S(1)}, bf16[2,4096,256]{2,1,0:T(8,128)(2,1)}, u32[]{:S(2)}) copy-start(bf16[2,4096,256]{2,1,0:T(8,128)(2,1)} %param.10) | copy-start | bytes 12582916
  58.3 8.9 %copy-start.2 = (bf16[384,512]{1,0:T(8,128)(2,1)}, bf16[384,512]{1,0:T(8,128)(2,1)S(1)}, u32[]{:S(2)}) copy-start(bf16[384,512]{1,0:T(8,128)(2,1)S(1)} %convolution_convert_fusion) | copy-start | bytes 1179652
  58.3 7.1 %collective-permute-start = (bf16[8,512]{1,0:T(8,128)(2,1)S(1)}, bf16[8,512]{1,0:T(8,128)(2,1)S(1)}, u32[]{:S(2)}, u32[]{:S(2)}) collective-permute-start(bf16[8,512]{1,0:T(8,128)(2,1)S(1)} %get-tuple-element.6), channel_id=1, source_target_pairs={{0,4},{4,8},{8,12},{12,16},{16,20},{20,24},{24,28},{1,5},{5,9},{9,... | collective-permute-start | bytes 24584 | tf_op jit(solution)/shard_map/ppermute | solution.py:17
  61.6 5.5 %collective-permute-start.1 = (bf16[8,512]{1,0:T(8,128)(2,1)S(1)}, bf16[8,512]{1,0:T(8,128)(2,1)S(1)}, u32[]{:S(2)}, u32[]{:S(2)}) collective-permute-start(bf16[8,512]{1,0:T(8,128)(2,1)S(1)} %get-tuple-element.7), channel_id=1, source_target_pairs={{4,0},{8,4},{12,8},{16,12},{20,16},{24,20},{28,24},{5,1},{9,5},{13... | collective-permute-start | bytes 24584 | tf_op jit(solution)/shard_map/ppermute | solution.py:18
  170.9 10.4 %copy-start.7 = (f32[4]{0:T(128)S(1)}, f32[4]{0:T(128)}, u32[]{:S(2)}) copy-start(f32[4]{0:T(128)} %param.14) | copy-start | bytes 52
  170.9 10.6 %copy-start.8 = (f32[128]{0:T(128)S(1)}, f32[128]{0:T(128)}, u32[]{:S(2)}) copy-start(f32[128]{0:T(128)} %param.15) | copy-start | bytes 1540
  171.0 10.8 %copy-start = (bf16[512,4096]{1,0:T(8,128)(2,1)S(1)}, bf16[512,4096]{1,0:T(8,128)(2,1)}, u32[]{:S(2)}) copy-start(bf16[512,4096]{1,0:T(8,128)(2,1)} %param.16) | copy-start | bytes 12582916
  181.7 2.0 copy-start.1
  181.7 2.0 copy-start.3
  181.7 2.0 copy-start.4
  181.7 2.0 copy-start.5
  181.8 2.0 copy-start.6
  181.8 2.6 %copy-start.10 = (bf16[512,4096]{1,0:T(8,128)(2,1)S(1)}, bf16[512,4096]{1,0:T(8,128)(2,1)}, u32[]{:S(2)}) copy-start(bf16[512,4096]{1,0:T(8,128)(2,1)} %param.17) | copy-start | bytes 12582916
  181.8 2.5 %copy-start.12 = (pred[512]{0:T(512)(128)(4,1)S(1)}, pred[512]{0:T(512)(128)(4,1)}, u32[]{:S(2)}) copy-start(pred[512]{0:T(512)(128)(4,1)} %get-tuple-element.16) | copy-start | bytes 1540
  181.8 2.5 %copy-start.13 = (pred[512]{0:T(512)(128)(4,1)S(1)}, pred[512]{0:T(512)(128)(4,1)}, u32[]{:S(2)}) copy-start(pred[512]{0:T(512)(128)(4,1)} %get-tuple-element.17) | copy-start | bytes 1540
  181.8 2.5 %copy-start.14 = (pred[512]{0:T(512)(128)(4,1)S(1)}, pred[512]{0:T(512)(128)(4,1)}, u32[]{:S(2)}) copy-start(pred[512]{0:T(512)(128)(4,1)} %get-tuple-element.18) | copy-start | bytes 1540
  181.8 2.5 %copy-start.15 = (pred[512]{0:T(512)(128)(4,1)S(1)}, pred[512]{0:T(512)(128)(4,1)}, u32[]{:S(2)}) copy-start(pred[512]{0:T(512)(128)(4,1)} %get-tuple-element.19) | copy-start | bytes 1540
Sparse Core Ops, SparseCore 0:
  9.5 31.2 all-gather.3
  46.8 60.0 all-gather.7
  109.0 58.6 all-gather.5
  189.8 36.5 reduce-scatter.1
where the time goes:
time: 233 us
  waiting for transfers between devices  129 us (55%)
  matrix products  49.9 us (21%)
  other arithmetic  27.8 us (12%)
  between operations  14.1 us (6%)
  local copies, waits for them, and re-layouts  6.99 us (3%)
  starting transfers between devices  4.79 us (2%)
    all_gather x1, waiting for transfers between devices, on_device(): key_piece = lax.all_gather(keys, 'sp', axis=0, tiled=True)  38.6 us
    reduce_scatter x1, waiting for transfers between devices, on_device(): lax.psum_scatter((jnp.dot(attn, attn_out_weight, preferred_element_type=j...  36.1 us
    all_gather x1, waiting for transfers between devices, on_device(): piece = lax.all_gather(inputs, 'tp', axis=1, tiled=True)  32.9 us
    convert_element_type x1, other arithmetic, on_device(): expo.astype(jnp.bfloat16)  23.4 us
    all_gather x1, waiting for transfers between devices, on_device(): value_piece = lax.all_gather(values, 'sp', axis=0, tiled=True)  19.2 us
    dot_general x1, matrix products, on_device(): jnp.einsum('qmhd,kmhd->mhqk', queries, key_heads, preferred_element_type=...  15.1 us
    dot_general x1, matrix products, on_device(): jnp.einsum('mhqk,khe->mhqe', expo.astype(jnp.bfloat16), value_heads, pref...  10.3 us
    dot_general x1, matrix products, on_device(): jnp.einsum('td,mdc->tmc', piece, key_weight, preferred_element_type=jnp.f...  5.82 us
  transfers between devices with their start and end apart: 6, of which 5 were waited for; matrix products, arithmetic and copies ran while one was open for 25% of the time, Pallas kernels for 0%

commit v1 on v0

v1 whole, which is shorter than its diff:
```python
import functools

import jax
import jax.numpy as jnp
from jax import lax
from jax.experimental import pallas as pl
from jax.experimental.pallas import tpu as pltpu
from jax.sharding import PartitionSpec as P

HEAD_DIM = 64
POOL_WIDTH = 2048
HALO = 16
F32 = jnp.float32
BF16 = jnp.bfloat16


def dot(a, b):
    return jnp.dot(a, b, preferred_element_type=F32)


def dot_t(a, b):
    return lax.dot_general(a, b, (((1,), (1,)), ((), ())), preferred_element_type=F32)


def kernel(
    S, T, NC, NCC, TQ, KB,
    x_ref, wq, wk, wv, wp, lam_ref, gain_ref, wa, wb,
    out_ref, lt_out,
    w, wo, xg, acc, kvst, qst, kv, qbuf, pin, halo, cat, ost, ltc, ltst, ltr, part, prs, yst, yrs,
    w_sem, wo_sem, xp_s, xp_r, xy_s, xy_r, xf_s, xf_r, a_s, a_r, q_s, q_r, loc, f_s, f_r,
    h_s, h_r, o_s, o_r, l_s, l_r, p_s, p_r, y_s, y_r,
):
    tok, F = x_ref.shape
    C = wq.shape[2]
    Cp = wp.shape[1]
    H = C // HEAD_DIM
    E = 2 * HEAD_DIM
    D = wa.shape[1]
    R = S // H
    Y = T // 2
    rows = tok // NC
    rb = tok // T
    s = lax.axis_index("sp")
    t = lax.axis_index("tp")
    g, r = s // R, s % R
    y, c = t // 2, t % 2
    partner = y * 2 + (1 - c)

    def w_copies(k):
        blk = (y * 2 + c) if k == 0 else (partner if k == 1 else None)
        if k >= 2:
            blk = ((y + k // 2) % Y) * 2 + (c if k % 2 == 0 else 1 - c)
        rs = pl.ds(pl.multiple_of(blk * F, F), F)
        out = []
        for i, (src, lo, n) in enumerate((
            (wk.at[0, rs, :], 2 * C, C), (wk.at[1, rs, :], 3 * C, C),
            (wv.at[rs, :], 4 * C, 2 * C),
            (wq.at[0, rs, :], 0, C), (wq.at[1, rs, :], C, C),
            (wp.at[rs, :], 6 * C, Cp),
        )):
            out.append(pltpu.make_async_copy(src, w.at[rs, lo:lo + n], w_sem.at[k, i]))
        return out

    for k in range(T):
        for cp in w_copies(k):
            cp.start()
    wo_cp = [
        pltpu.make_async_copy(wa, wo.at[0:H * E, :], wo_sem.at[0]),
        pltpu.make_async_copy(wb, wo.at[H * E:H * E + Cp, :], wo_sem.at[1]),
    ]

    bar = pltpu.get_barrier_semaphore()
    peers = [{"tp": partner}]
    peers += [{"tp": ((y + k) % Y) * 2 + c} for k in range(1, Y)]
    peers += [{"sp": ((g + k) % H) * R + r} for k in range(1, H)]
    peers += [{"sp": g * R + (r + j) % R} for j in range(1, R)]
    peers += [{"sp": (s + 1) % S}, {"sp": (s + S - 1) % S}]
    for d in peers:
        pl.semaphore_signal(bar, inc=1, device_id=d, device_id_type=pl.DeviceIdType.MESH)
    pl.semaphore_wait(bar, len(peers))

    def rc(src, dst, ss, rs, dev):
        return pltpu.make_async_remote_copy(
            src_ref=src, dst_ref=dst, send_sem=ss, recv_sem=rs,
            device_id=dev, device_id_type=pl.DeviceIdType.MESH)

    def ch(i):
        return pl.ds(i * rows, rows)

    xy = {}
    for i in range(NC):
        for k in range(1, Y):
            cp = rc(x_ref.at[ch(i), :], xg.at[t, ch(i), :], xy_s.at[k - 1, i], xy_r.at[k - 1, i],
                    {"tp": ((y + k) % Y) * 2 + c})
            cp.start()
            xy[k, i] = cp
    xp = rc(x_ref, xg.at[t], xp_s, xp_r, {"tp": partner})
    xp.start()
    for cp in wo_cp:
        cp.start()

    own_rows = pl.ds(pl.multiple_of(t * F, F), F)
    par_rows = pl.ds(pl.multiple_of(partner * F, F), F)
    N = 6 * C + Cp
    NT = 2 * C
    for cp in w_copies(0):
        cp.wait()

    @pl.loop(0, N // NT)
    def _(i):
        col = pl.ds(pl.multiple_of(i * NT, NT), NT)
        acc[:, col] = dot(x_ref[...], w[own_rows, col])

    for cp in w_copies(1):
        cp.wait()
    xp.wait_recv()

    @pl.loop(0, N // NT)
    def _(i):
        col = pl.ds(pl.multiple_of(i * NT, NT), NT)
        acc[:, col] += dot(xg[partner], w[par_rows, col])

    lane = lax.broadcasted_iota(jnp.int32, (rows, E), 1)
    low = lane < HEAD_DIM

    def pack(val, h):
        lo = (h // 2) * E
        a, b = val[:, lo:lo + E], val[:, C + lo:C + lo + E]
        if h % 2 == 0:
            return jnp.where(low, a, pltpu.roll(b, HEAD_DIM, 1)).astype(BF16)
        return jnp.where(low, pltpu.roll(a, HEAD_DIM, 1), b).astype(BF16)

    def kvrows(blk, i):
        return pl.ds(pl.multiple_of(blk * tok + i * rows, rows), rows)

    def forward(i):
        cps = []
        for k in range(1, H):
            src_blk = ((g + H - k) % H) * R + r
            zc[k, i].wait_recv()
            for j in range(1, R):
                cp = rc(kv.at[kvrows(src_blk, i), :], kv.at[kvrows(src_blk, i), :],
                        f_s.at[k, j - 1, i], f_r.at[k, j - 1, i], {"sp": g * R + (r + j) % R})
                cp.start()
                cps.append(cp)
        return cps

    zc, zq, xf, fwd, local = {}, {}, {}, [], []
    for i in range(NC):
        for k in range(1, Y):
            src = ((y + Y - k) % Y) * 2 + c
            xy[k, i].wait_recv()
            cp = rc(xg.at[src, ch(i), :], xg.at[src, ch(i), :], xf_s.at[k - 1, i], xf_r.at[k - 1, i],
                    {"tp": partner})
            cp.start()
            xf[k, i] = cp
        if i == 0:
            for k in range(2, T):
                for cp in w_copies(k):
                    cp.wait()
        for k in range(1, Y):
            xf[k, i].wait_recv()

        def section(lo, n):
            val = acc[ch(i), lo:lo + n]
            for k in range(1, Y):
                for cc in (c, 1 - c):
                    src = ((y + Y - k) % Y) * 2 + cc
                    val = val + dot(xg[src, ch(i), :], w[pl.ds(pl.multiple_of(src * F, F), F), lo:lo + n])
            return val

        kval = section(2 * C, 2 * C)
        for h in range(H):
            kvst[h, ch(i), 0:E] = pack(kval, h)
        vval = section(4 * C, 2 * C)
        for h in range(H):
            kvst[h, ch(i), E:2 * E] = vval[:, h * E:(h + 1) * E].astype(BF16)
        for k in range(1, H):
            gp = (g + k) % H
            cp = rc(kvst.at[gp, ch(i), :], kv.at[kvrows(s, i), :], a_s.at[k - 1, i], a_r.at[k - 1, i],
                    {"sp": gp * R + r})
            cp.start()
            zc[k, i] = cp
        for j in range(1, R):
            cp = rc(kvst.at[g, ch(i), :], kv.at[kvrows(s, i), :], f_s.at[0, j - 1, i], f_r.at[0, j - 1, i],
                    {"sp": g * R + (r + j) % R})
            cp.start()
            fwd.append(cp)
        cp = pltpu.make_async_copy(kvst.at[g, ch(i), :], kv.at[kvrows(s, i), :], loc.at[0, i])
        cp.start()
        local.append(cp)
        qval = section(0, 2 * C) * (HEAD_DIM ** -0.5)
        for h in range(H):
            qst[h, ch(i), :] = pack(qval, h)
        for k in range(1, H):
            gp = (g + k) % H
            cp = rc(qst.at[gp, ch(i), :], qbuf.at[g, ch(i), :], q_s.at[k - 1, i], q_r.at[k - 1, i],
                    {"sp": gp * R + r})
            cp.start()
            zq[k, i] = cp
        cp = pltpu.make_async_copy(qst.at[g, ch(i), :], qbuf.at[g, ch(i), :], loc.at[1, i])
        cp.start()
        local.append(cp)
        pin[pl.ds(HALO + i * rows, rows), :] = section(6 * C, Cp).astype(BF16)
        if i > 0:
            fwd += forward(i - 1)

    up = rc(pin.at[pl.ds(tok, HALO), :], halo.at[0], h_s.at[0], h_r.at[0], {"sp": (s + 1) % S})
    down = rc(pin.at[pl.ds(HALO, HALO), :], halo.at[1], h_s.at[1], h_r.at[1], {"sp": (s + S - 1) % S})
    up.start()
    down.start()
    fwd += forward(NC - 1)
    up.wait_recv()
    down.wait_recv()
    zero = jnp.zeros((HALO, Cp), BF16)
    pin[0:HALO, :] = jnp.where(s > 0, halo[0], zero)
    pin[pl.ds(HALO + tok, HALO), :] = jnp.where(s < S - 1, halo[1], zero)
    group = (t * Cp) // (POOL_WIDTH // 4)
    radius = jnp.where(group == 0, 1, jnp.where(group == 1, 2, jnp.where(group == 2, 4, 8)))
    ti = lax.broadcasted_iota(jnp.int32, (tok, tok + 2 * HALO), 0)
    ui = lax.broadcasted_iota(jnp.int32, (tok, tok + 2 * HALO), 1) - HALO
    band = jnp.where((ui >= ti - radius) & (ui < ti + radius), 1.0, 0.0).astype(BF16)
    pos = s * tok + lax.broadcasted_iota(jnp.int32, (tok, 1), 0)
    count = jnp.minimum(pos + radius, S * tok) - jnp.maximum(pos - radius, 0)
    mean = dot(band, pin[...]) / count.astype(F32)
    cat[:, H * E:H * E + Cp] = (mean - pin[HALO:HALO + tok, :].astype(F32)).astype(BF16)

    for cp in local:
        cp.wait()
    for i in range(NC):
        for k in range(1, H):
            zq[k, i].wait_recv()
    for cp in fwd:
        cp.wait_recv()
    lam = lam_ref[g]
    gain = gain_ref[...]
    qlow = lax.broadcasted_iota(jnp.int32, (TQ, E), 1) < HEAD_DIM
    llane = lax.broadcasted_iota(jnp.int32, (TQ, E), 1) % 2 == 0
    nk = (S * tok) // KB

    def scores(q2, ks):
        return dot_t(q2, kv[ks, 0:E])

    oc, lc = {}, {}
    for k in [*range(1, H), 0]:
        gp = (g + k) % H

        @pl.loop(0, tok // TQ)
        def _(i, gp=gp):
            rr = pl.ds(pl.multiple_of(i * TQ, TQ), TQ)
            q = qbuf[gp, rr, :]
            z = jnp.zeros_like(q)
            q2 = jnp.concatenate([jnp.where(qlow, q, z), jnp.where(qlow, z, q)], axis=0)

            def block(b, carry):
                ks = pl.ds(pl.multiple_of(b * KB, KB), KB)
                sc = scores(q2, ks)
                bm = jnp.max(sc, axis=1, keepdims=True)
                if carry is None:
                    p = jnp.exp(sc - bm)
                    return bm, jnp.sum(p, axis=1, keepdims=True), dot(p.astype(BF16), kv[ks, E:2 * E])
                m, tt, n = carry
                nm = jnp.maximum(m, bm)
                old = jnp.exp(m - nm)
                p = jnp.exp(sc - nm)
                return (nm, tt * old + jnp.sum(p, axis=1, keepdims=True),
                        n * old + dot(p.astype(BF16), kv[ks, E:2 * E]))

            carry = block(0, None)
            if nk > 1:
                carry = lax.fori_loop(1, nk, block, carry)
            m, tt, n = carry
            n = n / tt
            lt = m + jnp.log(tt)
            diff = n[:TQ] - lam * n[TQ:]
            o = diff * lax.rsqrt(jnp.mean(diff * diff, axis=1, keepdims=True) + 1e-05) * gain
            ost[gp, rr, :] = o.astype(BF16)
            ltc[rr, :] = jnp.where(llane, lt[:TQ], lt[TQ:])

        ltst[gp] = jnp.transpose(ltc[...])[0:8, :]
        ocol = pl.ds(pl.multiple_of(g * E, E), E)
        if k > 0:
            dev = {"sp": gp * R + r}
            oc[k] = rc(ost.at[gp], cat.at[:, ocol], o_s.at[k - 1], o_r.at[k - 1], dev)
            lc[k] = rc(ltst.at[gp], ltr.at[g], l_s.at[k - 1], l_r.at[k - 1], dev)
            oc[k].start()
            lc[k].start()
        else:
            a = pltpu.make_async_copy(ost.at[gp], cat.at[:, ocol], loc.at[0, 0])
            b = pltpu.make_async_copy(ltst.at[gp], ltr.at[g], loc.at[1, 0])
            a.start()
            b.start()
            a.wait()
            b.wait()

    for cp in wo_cp:
        cp.wait()
    for k in range(1, H):
        oc[k].wait_recv()

    W = D // NCC
    pc, yc = {}, {}
    for i in range(NCC):
        cols = slice(i * W, (i + 1) * W)
        part[:, cols] = dot(cat[...], wo[:, cols]).astype(BF16)
        for yy in range(Y):
            src = pl.ds(pl.multiple_of((yy * 2 + 1 - c) * rb, rb), rb)
            pc[i, yy] = rc(part.at[src, cols], prs.at[yy, :, cols], p_s.at[i, yy], p_r.at[i, yy], {"tp": partner})
            pc[i, yy].start()

    def pair(yy, cols):
        mine = pl.ds(pl.multiple_of((yy * 2 + c) * rb, rb), rb)
        return part[mine, cols].astype(F32) + prs[yy, :, cols].astype(F32)

    for i in range(NCC):
        cols = slice(i * W, (i + 1) * W)
        for yy in range(Y):
            pc[i, yy].wait_recv()
        for k in range(1, Y):
            yd = (y + k) % Y
            yst[k - 1, :, cols] = pair(yd, cols).astype(BF16)
            yc[k, i] = rc(yst.at[k - 1, :, cols], yrs.at[k - 1, :, cols], y_s.at[k - 1, i], y_r.at[k - 1, i],
                          {"tp": yd * 2 + c})
            yc[k, i].start()
    for k in range(1, H):
        lc[k].wait_recv()
    for h in range(H):
        lt_out[0, h:h + 1, :] = ltr[h, 0:1, :]
        lt_out[1, h:h + 1, :] = ltr[h, 1:2, :]
    for i in range(NCC):
        cols = slice(i * W, (i + 1) * W)
        val = pair(y, cols)
        for k in range(1, Y):
            yc[k, i].wait_recv()
            val = val + yrs[k - 1, :, cols].astype(F32)
        out_ref[:, cols] = val.astype(BF16)

    sends = [xp, *xy.values(), *xf.values(), *zc.values(), *zq.values(), *fwd, up, down,
             *oc.values(), *lc.values(), *pc.values(), *yc.values()]
    for cp in sends:
        cp.wait_send()


def solution(mesh):
    S, T = mesh.shape["sp"], mesh.shape["tp"]

    def on_device(x, wq, wk, wv, wp, lam, gain, wa, wb):
        tok, F = x.shape
        D, C = wq.shape[1:]
        Cp = wp.shape[1]
        H = C // HEAD_DIM
        E = 2 * HEAD_DIM
        R, Y = S // H, T // 2
        NC, NCC = 3, 4
        TQ = 128
        KB = min(S * tok, 3072)
        rb = tok // T
        N = 6 * C + Cp
        vm = pltpu.VMEM
        dma = pltpu.SemaphoreType.DMA
        scratch = [
            vm((D, N), BF16), vm((H * E + Cp, D), BF16), vm((T, tok, F), BF16), vm((tok, N), F32),
            vm((H, tok, 2 * E), BF16), vm((H, tok, E), BF16), vm((S * tok, 2 * E), BF16), vm((H, tok, E), BF16),
            vm((tok + 2 * HALO, Cp), BF16), vm((2, HALO, Cp), BF16), vm((tok, H * E + Cp), BF16),
            vm((H, tok, E), BF16), vm((tok, E), F32), vm((H, 8, tok), F32), vm((H, 8, tok), F32),
            vm((tok, D), BF16), vm((Y, rb, D), BF16), vm((Y - 1, rb, D), BF16), vm((Y - 1, rb, D), BF16),
            dma((T, 6)), dma((2,)), dma, dma, dma((Y - 1, NC)), dma((Y - 1, NC)), dma((Y - 1, NC)), dma((Y - 1, NC)),
            dma((H - 1, NC)), dma((H - 1, NC)), dma((H - 1, NC)), dma((H - 1, NC)), dma((2, NC)),
            dma((H, R - 1, NC)), dma((H, R - 1, NC)), dma((2,)), dma((2,)),
            dma((H - 1,)), dma((H - 1,)), dma((H - 1,)), dma((H - 1,)),
            dma((NCC, Y)), dma((NCC, Y)), dma((Y - 1, NCC)), dma((Y - 1, NCC)),
        ]
        vspec = pl.BlockSpec(memory_space=pltpu.VMEM)
        aspec = pl.BlockSpec(memory_space=pl.ANY)
        return pl.pallas_call(
            functools.partial(kernel, S, T, NC, NCC, TQ, KB),
            out_shape=(jax.ShapeDtypeStruct((rb, D), BF16), jax.ShapeDtypeStruct((2, H, tok), F32)),
            in_specs=[vspec, aspec, aspec, aspec, aspec, pl.BlockSpec(memory_space=pltpu.SMEM), vspec, aspec, aspec],
            out_specs=(vspec, vspec),
            scratch_shapes=scratch,
            compiler_params=pltpu.CompilerParams(
                collective_id=0, has_side_effects=True, vmem_limit_bytes=67043328),
        )(x, wq, wk, wv, wp, lam, gain.reshape(1, E), wa, wb)

    in_specs = (
        P("sp", "tp"), P(None, None, "tp"), P(None, None, "tp"), P(None, "tp"), P(None, "tp"),
        P("tp"), P(), P("tp", None), P("tp", None),
    )
    out_specs = (P(("sp", "tp"), None), P(None, "tp", "sp"))
    return jax.shard_map(on_device, mesh=mesh, in_specs=in_specs, out_specs=out_specs, check_vma=False)
```

time: 233 us -> 94.1 us (0.40)
  waiting for transfers between devices: 129 us -> 0 us
  Pallas kernels: 0 us -> 89.8 us
  matrix products: 49.9 us -> 0 us
  other arithmetic: 27.8 us -> 0 us
  between operations: 14.1 us -> 0.64 us
  starting transfers between devices: 4.79 us -> 0 us
  local copies, waits for them, and re-layouts: 6.99 us -> 3.37 us
    all_gather x3 -> x0, waiting for transfers between devices: 90.7 us -> none  [the longest x1 38.6 us: on_device(): key_piece = lax.all_gather(keys, 'sp', axis=0, tiled=True)]
    pallas_call x0 -> x1, Pallas kernels: none -> 89.8 us  [on_device(): pl.pallas_call(functools.partial(kernel, S, T, NC, NCC, TQ, KB), out_shap...]
    dot_general x8 -> x0, matrix products: 49.9 us -> none  [the longest x1 15.1 us: on_device(): jnp.einsum('qmhd,kmhd->mhqk', queries, key_heads, preferred_element_type=...]
    reduce_scatter x1 -> x0, waiting for transfers between devices: 36.1 us -> none  [on_device(): lax.psum_scatter((jnp.dot(attn, attn_out_weight, preferred_element_type=j...]
    convert_element_type x5 -> x0, other arithmetic: 25.8 us -> none  [the longest x1 23.4 us: on_device(): expo.astype(jnp.bfloat16)]
    ppermute x2 -> x0, starting transfers between devices: 4.63 us -> none  [the longest x1 3.34 us: extended(): before = lax.ppermute(last, axis, up)]
    all_gather x1 -> x0, local copies, waits for them, and re-layouts: 3.18 us -> none  [on_device(): key_piece = lax.all_gather(keys, 'sp', axis=0, tiled=True)]
    reshape x1 -> x0, local copies, waits for them, and re-layouts: 3.18 us -> none  [on_device(): value_heads = value_piece.reshape(rows, heads_here, 2 * HEAD_DIM)]
  transfers between devices with their start and end apart: 6 -> 0, of which waited for: 5 -> 0; matrix products, arithmetic and copies ran while one was open for 25% -> 0% of each run, Pallas kernels for 0% -> 0%
where the time goes in v1:
time: 94.1 us; the launch traced here: 93.8 us
  Pallas kernels  89.8 us (95%)
  local copies, waits for them, and re-layouts  3.37 us (4%)
    pallas_call x1, Pallas kernels, on_device(): pl.pallas_call(functools.partial(kernel, S, T, NC, NCC, TQ, KB), out_shap...  89.8 us
    unnamed x2, local copies, waits for them, and re-layouts  3.37 us

profile of v1, /device:TPU:0, one launch (start us, length us, event | category | flops | bytes accessed | tf_op | source)
XLA Modules:
  0.0 93.8 jit_solution(10264672721204452659)
XLA Ops:
  0.6 89.8 %shard_map.104 = (bf16[96,4096]{1,0:T(8,128)(2,1)}, f32[2,4,384]{2,1,0:T(4,128)}) custom-call(bf16[384,1024]{1,0:T(8,128)(2,1)} %x_ref.1, bf16[2,4096,256]{2,1,0:T(8,128)(2,1)} %wq.1, bf16[2,4096,256]{2,1,0:T(8,128)(2,1)} %wk.1, bf16[4096,512]{1,0:T(8,128)(2,1)} %wv.1, bf16[4096,512]{1,0:T(8,128)(2,1)} %wp.1, f32[4]{0:T(128)} %lam_ref.1, f32[1,128]{1,0:T(1,128)} %bitcast.1, ...), custom_call_target="tpu_custom_call" | custom-call | tf_op jit(solution)/shard_map/pallas_call | solution.py:375
  90.5 2.1 %copy.13 = bf16[96,4096]{1,0:T(8,128)(2,1)} copy(bf16[96,4096]{1,0:T(8,128)(2,1)} %get-tuple-element.4) | data formatting | bytes 1572864
  92.5 1.3 %copy.14 = f32[2,4,384]{2,1,0:T(4,128)} copy(f32[2,4,384]{2,1,0:T(4,128)} %get-tuple-element.5) | data formatting | bytes 24576

commit v2 on v1

--- a/solution.py
+++ b/solution.py
@@ -23,12 +23,12 @@
 
 
 def kernel(
-    S, T, NC, NCC, TQ, KB,
+    S, T, NC, NCC, PS, KB,
     x_ref, wq, wk, wv, wp, lam_ref, gain_ref, wa, wb,
     out_ref, lt_out,
     w, wo, xg, acc, kvst, qst, kv, qbuf, pin, halo, cat, ost, ltc, ltst, ltr, part, prs, yst, yrs,
     w_sem, wo_sem, xp_s, xp_r, xy_s, xy_r, xf_s, xf_r, a_s, a_r, q_s, q_r, loc, f_s, f_r,
-    h_s, h_r, o_s, o_r, l_s, l_r, p_s, p_r, y_s, y_r,
+    h_s, h_r, oloc, o_s, o_r, l_s, l_r, p_s, p_r, y_s, y_r,
 ):
     tok, F = x_ref.shape
     C = wq.shape[2]
@@ -204,6 +204,11 @@
         pin[pl.ds(HALO + i * rows, rows), :] = section(6 * C, Cp).astype(BF16)
         if i > 0:
             fwd += forward(i - 1)
+
+    starts = [sum(PS[:p]) for p in range(len(PS))]
+
+    def place(p, j):
+        return j * rb + starts[p], T * starts[p] + j * PS[p]
 
     up = rc(pin.at[pl.ds(tok, HALO), :], halo.at[0], h_s.at[0], h_r.at[0], {"sp": (s + 1) % S})
     down = rc(pin.at[pl.ds(HALO, HALO), :], halo.at[1], h_s.at[1], h_r.at[1], {"sp": (s + S - 1) % S})
@@ -223,7 +228,11 @@
     pos = s * tok + lax.broadcasted_iota(jnp.int32, (tok, 1), 0)
     count = jnp.minimum(pos + radius, S * tok) - jnp.maximum(pos - radius, 0)
     mean = dot(band, pin[...]) / count.astype(F32)
-    cat[:, H * E:H * E + Cp] = (mean - pin[HALO:HALO + tok, :].astype(F32)).astype(BF16)
+    pooled = (mean - pin[HALO:HALO + tok, :].astype(F32)).astype(BF16)
+    for p in range(len(PS)):
+        for j in range(T):
+            nat, per = place(p, j)
+            cat[per:per + PS[p], H * E:H * E + Cp] = pooled[nat:nat + PS[p], :]
 
     for cp in local:
         cp.wait()
@@ -234,109 +243,130 @@
         cp.wait_recv()
     lam = lam_ref[g]
     gain = gain_ref[...]
-    qlow = lax.broadcasted_iota(jnp.int32, (TQ, E), 1) < HEAD_DIM
-    llane = lax.broadcasted_iota(jnp.int32, (TQ, E), 1) % 2 == 0
     nk = (S * tok) // KB
-
-    def scores(q2, ks):
-        return dot_t(q2, kv[ks, 0:E])
-
-    oc, lc = {}, {}
-    for k in [*range(1, H), 0]:
+    oc, lc, pc, yc = {}, {}, {}, {}
+    ocol = pl.ds(pl.multiple_of(g * E, E), E)
+    W = D // NCC
+
+    def attend(p, k):
+        n = T * PS[p]
         gp = (g + k) % H
-
-        @pl.loop(0, tok // TQ)
-        def _(i, gp=gp):
-            rr = pl.ds(pl.multiple_of(i * TQ, TQ), TQ)
-            q = qbuf[gp, rr, :]
-            z = jnp.zeros_like(q)
-            q2 = jnp.concatenate([jnp.where(qlow, q, z), jnp.where(qlow, z, q)], axis=0)
-
-            def block(b, carry):
-                ks = pl.ds(pl.multiple_of(b * KB, KB), KB)
-                sc = scores(q2, ks)
-                bm = jnp.max(sc, axis=1, keepdims=True)
-                if carry is None:
-                    p = jnp.exp(sc - bm)
-                    return bm, jnp.sum(p, axis=1, keepdims=True), dot(p.astype(BF16), kv[ks, E:2 * E])
-                m, tt, n = carry
-                nm = jnp.maximum(m, bm)
-                old = jnp.exp(m - nm)
-                p = jnp.exp(sc - nm)
-                return (nm, tt * old + jnp.sum(p, axis=1, keepdims=True),
-                        n * old + dot(p.astype(BF16), kv[ks, E:2 * E]))
-
-            carry = block(0, None)
-            if nk > 1:
-                carry = lax.fori_loop(1, nk, block, carry)
-            m, tt, n = carry
-            n = n / tt
-            lt = m + jnp.log(tt)
-            diff = n[:TQ] - lam * n[TQ:]
-            o = diff * lax.rsqrt(jnp.mean(diff * diff, axis=1, keepdims=True) + 1e-05) * gain
-            ost[gp, rr, :] = o.astype(BF16)
-            ltc[rr, :] = jnp.where(llane, lt[:TQ], lt[TQ:])
-
-        ltst[gp] = jnp.transpose(ltc[...])[0:8, :]
-        ocol = pl.ds(pl.multiple_of(g * E, E), E)
+        pr = slice(T * starts[p], T * starts[p] + n)
+        qlow = lax.broadcasted_iota(jnp.int32, (n, E), 1) < HEAD_DIM
+        even = lax.broadcasted_iota(jnp.int32, (n, E), 1) % 2 == 0
+        q = jnp.concatenate([qbuf[gp, j * rb + starts[p]:j * rb + starts[p] + PS[p], :] for j in range(T)], axis=0)
+        z = jnp.zeros_like(q)
+        q2 = jnp.concatenate([jnp.where(qlow, q, z), jnp.where(qlow, z, q)], axis=0)
+
+        def block(b, carry):
+            ks = pl.ds(pl.multiple_of(b * KB, KB), KB)
+            sc = dot_t(q2, kv[ks, 0:E])
+            bm = jnp.max(sc, axis=1, keepdims=True)
+            if carry is None:
+                e = jnp.exp(sc - bm)
+                return bm, jnp.sum(e, axis=1, keepdims=True), dot(e.astype(BF16), kv[ks, E:2 * E])
+            m, tt, num = carry
+            nm = jnp.maximum(m, bm)
+            old = jnp.exp(m - nm)
+            e = jnp.exp(sc - nm)
+            return (nm, tt * old + jnp.sum(e, axis=1, keepdims=True),
+                    num * old + dot(e.astype(BF16), kv[ks, E:2 * E]))
+
+        carry = block(0, None)
+        if nk > 1:
+            carry = lax.fori_loop(1, nk, block, carry)
+        m, tt, num = carry
+        num = num / tt
+        lt = m + jnp.log(tt)
+        diff = num[:n] - lam * num[n:]
+        o = diff * lax.rsqrt(jnp.mean(diff * diff, axis=1, keepdims=True) + 1e-05) * gain
+        ost[gp, pr, :] = o.astype(BF16)
+        both = jnp.where(even, lt[:n], lt[n:])
+        for j in range(T):
+            nat, per = place(p, j)
+            ltc[gp, nat:nat + PS[p], :] = both[j * PS[p]:(j + 1) * PS[p]]
         if k > 0:
-            dev = {"sp": gp * R + r}
-            oc[k] = rc(ost.at[gp], cat.at[:, ocol], o_s.at[k - 1], o_r.at[k - 1], dev)
-            lc[k] = rc(ltst.at[gp], ltr.at[g], l_s.at[k - 1], l_r.at[k - 1], dev)
-            oc[k].start()
-            lc[k].start()
+            oc[k, p] = rc(ost.at[gp, pr, :], cat.at[pr, ocol], o_s.at[k - 1, p], o_r.at[k - 1, p], {"sp": gp * R + r})
+            oc[k, p].start()
         else:
-            a = pltpu.make_async_copy(ost.at[gp], cat.at[:, ocol], loc.at[0, 0])
-            b = pltpu.make_async_copy(ltst.at[gp], ltr.at[g], loc.at[1, 0])
-            a.start()
-            b.start()
-            a.wait()
-            b.wait()
-
-    for cp in wo_cp:
-        cp.wait()
-    for k in range(1, H):
-        oc[k].wait_recv()
-
-    W = D // NCC
-    pc, yc = {}, {}
-    for i in range(NCC):
-        cols = slice(i * W, (i + 1) * W)
-        part[:, cols] = dot(cat[...], wo[:, cols]).astype(BF16)
-        for yy in range(Y):
-            src = pl.ds(pl.multiple_of((yy * 2 + 1 - c) * rb, rb), rb)
-            pc[i, yy] = rc(part.at[src, cols], prs.at[yy, :, cols], p_s.at[i, yy], p_r.at[i, yy], {"tp": partner})
-            pc[i, yy].start()
-
-    def pair(yy, cols):
-        mine = pl.ds(pl.multiple_of((yy * 2 + c) * rb, rb), rb)
-        return part[mine, cols].astype(F32) + prs[yy, :, cols].astype(F32)
-
-    for i in range(NCC):
-        cols = slice(i * W, (i + 1) * W)
-        for yy in range(Y):
-            pc[i, yy].wait_recv()
-        for k in range(1, Y):
-            yd = (y + k) % Y
-            yst[k - 1, :, cols] = pair(yd, cols).astype(BF16)
-            yc[k, i] = rc(yst.at[k - 1, :, cols], yrs.at[k - 1, :, cols], y_s.at[k - 1, i], y_r.at[k - 1, i],
-                          {"tp": yd * 2 + c})
-            yc[k, i].start()
+            cp = pltpu.make_async_copy(ost.at[gp, pr, :], cat.at[pr, ocol], oloc.at[p])
+            cp.start()
+            oc[k, p] = cp
+        if p == len(PS) - 1:
+            ltst[gp] = jnp.transpose(ltc[gp])[0:8, :]
+            if k > 0:
+                lc[k] = rc(ltst.at[gp], ltr.at[g], l_s.at[k - 1], l_r.at[k - 1], {"sp": gp * R + r})
+                lc[k].start()
+            else:
+                ltr[g] = ltst[gp]
+
+    def project(p):
+        for k in range(1, H):
+            oc[k, p].wait_recv()
+        oc[0, p].wait()
+        pr = slice(T * starts[p], T * (starts[p] + PS[p]))
+        for i in range(NCC):
+            cols = slice(i * W, (i + 1) * W)
+            part[pr, cols] = dot(cat[pr, :], wo[:, cols]).astype(BF16)
+            for yy in range(Y):
+                src = pl.ds(pl.multiple_of(T * starts[p] + (yy * 2 + 1 - c) * PS[p], 16), PS[p])
+                cp = rc(part.at[src, cols], prs.at[yy, starts[p]:starts[p] + PS[p], cols],
+                        p_s.at[p, i, yy], p_r.at[p, i, yy], {"tp": partner})
+                cp.start()
+                pc[p, i, yy] = cp
+
+    def pair(p, yy, cols):
+        mine = pl.ds(pl.multiple_of(T * starts[p] + (yy * 2 + c) * PS[p], 16), PS[p])
+        return part[mine, cols].astype(F32) + prs[yy, starts[p]:starts[p] + PS[p], cols].astype(F32)
+
+    def cross(p):
+        dst = slice(starts[p], starts[p] + PS[p])
+        for i in range(NCC):
+            cols = slice(i * W, (i + 1) * W)
+            for yy in range(Y):
+                pc[p, i, yy].wait_recv()
+            for k in range(1, Y):
+                yd = (y + k) % Y
+                yst[k - 1, dst, cols] = pair(p, yd, cols).astype(BF16)
+                cp = rc(yst.at[k - 1, dst, cols], yrs.at[k - 1, dst, cols], y_s.at[k - 1, p, i], y_r.at[k - 1, p, i],
+                        {"tp": yd * 2 + c})
+                cp.start()
+                yc[k, p, i] = cp
+
+    def finish(p):
+        dst = slice(starts[p], starts[p] + PS[p])
+        for i in range(NCC):
+            cols = slice(i * W, (i + 1) * W)
+            val = pair(p, y, cols)
+            for k in range(1, Y):
+                yc[k, p, i].wait_recv()
+                val = val + yrs[k - 1, dst, cols].astype(F32)
+            out_ref[dst, cols] = val.astype(BF16)
+
+    order = [*range(1, H), 0]
+    for p in range(len(PS)):
+        for at, k in enumerate(order):
+            attend(p, k)
+            if p == 0 and at == 0:
+                for cp in wo_cp:
+                    cp.wait()
+            if p > 0 and at == (H - 1) // 2:
+                project(p - 1)
+            if p > 0 and at == max(H - 2, 0):
+                cross(p - 1)
+    last = len(PS) - 1
+    project(last)
+    cross(last)
     for k in range(1, H):
         lc[k].wait_recv()
     for h in range(H):
         lt_out[0, h:h + 1, :] = ltr[h, 0:1, :]
         lt_out[1, h:h + 1, :] = ltr[h, 1:2, :]
-    for i in range(NCC):
-        cols = slice(i * W, (i + 1) * W)
-        val = pair(y, cols)
-        for k in range(1, Y):
-            yc[k, i].wait_recv()
-            val = val + yrs[k - 1, :, cols].astype(F32)
-        out_ref[:, cols] = val.astype(BF16)
+    for p in range(len(PS)):
+        finish(p)
 
     sends = [xp, *xy.values(), *xf.values(), *zc.values(), *zq.values(), *fwd, up, down,
-             *oc.values(), *lc.values(), *pc.values(), *yc.values()]
+             *[v for q, v in oc.items() if q[0] > 0], *lc.values(), *pc.values(), *yc.values()]
     for cp in sends:
         cp.wait_send()
 
@@ -352,9 +382,11 @@
         E = 2 * HEAD_DIM
         R, Y = S // H, T // 2
         NC, NCC = 3, 4
-        TQ = 128
         KB = min(S * tok, 3072)
         rb = tok // T
+        NP = 3
+        big = -(-rb // (16 * NP)) * 16
+        PS = [min(big, rb - big * i) for i in range(NP)]
         N = 6 * C + Cp
         vm = pltpu.VMEM
         dma = pltpu.SemaphoreType.DMA
@@ -362,18 +394,18 @@
             vm((D, N), BF16), vm((H * E + Cp, D), BF16), vm((T, tok, F), BF16), vm((tok, N), F32),
             vm((H, tok, 2 * E), BF16), vm((H, tok, E), BF16), vm((S * tok, 2 * E), BF16), vm((H, tok, E), BF16),
             vm((tok + 2 * HALO, Cp), BF16), vm((2, HALO, Cp), BF16), vm((tok, H * E + Cp), BF16),
-            vm((H, tok, E), BF16), vm((tok, E), F32), vm((H, 8, tok), F32), vm((H, 8, tok), F32),
+            vm((H, tok, E), BF16), vm((H, tok, E), F32), vm((H, 8, tok), F32), vm((H, 8, tok), F32),
             vm((tok, D), BF16), vm((Y, rb, D), BF16), vm((Y - 1, rb, D), BF16), vm((Y - 1, rb, D), BF16),
             dma((T, 6)), dma((2,)), dma, dma, dma((Y - 1, NC)), dma((Y - 1, NC)), dma((Y - 1, NC)), dma((Y - 1, NC)),
             dma((H - 1, NC)), dma((H - 1, NC)), dma((H - 1, NC)), dma((H - 1, NC)), dma((2, NC)),
-            dma((H, R - 1, NC)), dma((H, R - 1, NC)), dma((2,)), dma((2,)),
-            dma((H - 1,)), dma((H - 1,)), dma((H - 1,)), dma((H - 1,)),
-            dma((NCC, Y)), dma((NCC, Y)), dma((Y - 1, NCC)), dma((Y - 1, NCC)),
+            dma((H, R - 1, NC)), dma((H, R - 1, NC)), dma((2,)), dma((2,)), dma((NP,)),
+            dma((H - 1, NP)), dma((H - 1, NP)), dma((H - 1,)), dma((H - 1,)),
+            dma((NP, NCC, Y)), dma((NP, NCC, Y)), dma((Y - 1, NP, NCC)), dma((Y - 1, NP, NCC)),
         ]
         vspec = pl.BlockSpec(memory_space=pltpu.VMEM)
         aspec = pl.BlockSpec(memory_space=pl.ANY)
         return pl.pallas_call(
-            functools.partial(kernel, S, T, NC, NCC, TQ, KB),
+            functools.partial(kernel, S, T, NC, NCC, PS, KB),
             out_shape=(jax.ShapeDtypeStruct((rb, D), BF16), jax.ShapeDtypeStruct((2, H, tok), F32)),
             in_specs=[vspec, aspec, aspec, aspec, aspec, pl.BlockSpec(memory_space=pltpu.SMEM), vspec, aspec, aspec],
             out_specs=(vspec, vspec),

time: 94.1 us -> 86.5 us (0.919)
  Pallas kernels: 89.8 us -> 82.3 us
    pallas_call x1, Pallas kernels: 89.8 us -> 82.3 us  [on_device(): pl.pallas_call(functools.partial(kernel, S, T, NC, NCC, PS, KB), out_shap...]
where the time goes in v2:
time: 86.5 us; the launch traced here: 86.3 us
  Pallas kernels  82.3 us (95%)
  local copies, waits for them, and re-layouts  3.37 us (4%)
    pallas_call x1, Pallas kernels, on_device(): pl.pallas_call(functools.partial(kernel, S, T, NC, NCC, PS, KB), out_shap...  82.3 us
    unnamed x2, local copies, waits for them, and re-layouts  3.37 us

profile of v2, /device:TPU:0, one launch (start us, length us, event | category | flops | bytes accessed | tf_op | source)
XLA Modules:
  0.0 86.3 jit_solution(3002330956876088756)
XLA Ops:
  0.6 82.3 %shard_map.104 = (bf16[96,4096]{1,0:T(8,128)(2,1)}, f32[2,4,384]{2,1,0:T(4,128)}) custom-call(bf16[384,1024]{1,0:T(8,128)(2,1)} %x_ref.1, bf16[2,4096,256]{2,1,0:T(8,128)(2,1)} %wq.1, bf16[2,4096,256]{2,1,0:T(8,128)(2,1)} %wk.1, bf16[4096,512]{1,0:T(8,128)(2,1)} %wv.1, bf16[4096,512]{1,0:T(8,128)(2,1)} %wp.1, f32[4]{0:T(128)} %lam_ref.1, f32[1,128]{1,0:T(1,128)} %bitcast.1, ...), custom_call_target="tpu_custom_call" | custom-call | tf_op jit(solution)/shard_map/pallas_call | solution.py:407
  82.9 2.1 %copy.13 = bf16[96,4096]{1,0:T(8,128)(2,1)} copy(bf16[96,4096]{1,0:T(8,128)(2,1)} %get-tuple-element.4) | data formatting | bytes 1572864
  85.0 1.3 %copy.14 = f32[2,4,384]{2,1,0:T(4,128)} copy(f32[2,4,384]{2,1,0:T(4,128)} %get-tuple-element.5) | data formatting | bytes 24576
